TPU v7x, 32 devices: a whole 2x2x4 slice. The times are simulated.
32 devices in a mesh: fs: 8 (over z, y), tp: 4 (over x, core).
Axes of the slice: x: 2, y: 2, z: 4, core: 2. Of those that a mesh axis runs over, the one named last changes fastest.
Arguments:
- hidden_in: bfloat16 [512, 4096], P(None, 'tp'), may hold values from -6 to 6
- up_act: bfloat16 [512, 12288], P('tp', 'fs'), may hold values from -6 to 6
- up_val: bfloat16 [512, 12288], P('tp', 'fs'), may hold values from -6 to 6
- cotangent: bfloat16 [512, 4096], P('tp'), may hold values from -6 to 6
- w_act: bfloat16 [4096, 12288], P('tp', 'fs'), may hold values from -0.09375 to 0.09375
- w_val: bfloat16 [4096, 12288], P('tp', 'fs'), may hold values from -0.09375 to 0.09375
- w_down: bfloat16 [12288, 4096], P('fs', 'tp'), may hold values from -0.0546875 to 0.0546875
- conv_act: bfloat16 [3, 12288], P(None, 'fs'), may hold values from -3 to 3
- conv_val: bfloat16 [3, 12288], P(None, 'fs'), may hold values from -3 to 3
- bias_act: bfloat16 [12288], P('fs'), may hold values from -3 to 3
- bias_val: bfloat16 [12288], P('fs'), may hold values from -3 to 3
Outputs:
- grad_input: bfloat16 [512, 4096], P(('tp', 'fs'))
- grad_w_act: float32 [4096, 12288], P('tp', 'fs')
- grad_w_val: float32 [4096, 12288], P('tp', 'fs')
- grad_w_down: float32 [12288, 4096], P('fs', 'tp')
- grad_conv_act: float32 [3, 12288], P(None, 'fs')
- grad_conv_val: float32 [3, 12288], P(None, 'fs')
- grad_bias_act: float32 [12288], P('fs')
- grad_bias_val: float32 [12288], P('fs')
- rows_act: float32 [4096], P('tp')
- rows_val: float32 [4096], P('tp')
- rows_down: float32 [12288], P('fs')
- conv_rows: float32 [2, 3], replicated
All inputs are finite; a program needn't handle non-finite values.
Results may differ from a plain program's by a relative error of at most 0.0057.
Values may be sent and summed in bfloat16 or wider, within the bound.
A program may use at most 128 MiB of HBM per device.

v0:
```python
import jax
import jax.numpy as jnp
from jax import lax
from jax.sharding import PartitionSpec as P


def passed_along(value, axis, by):
    length = lax.axis_size(axis)
    pairs = [(i, i + by) for i in range(length) if 0 <= i + by < length]
    return lax.ppermute(value, axis, pairs)


def contract_last(left, right):
    return lax.dot_general(
        left, right, (((1,), (1,)), ((), ())), preferred_element_type=jnp.float32
    )


def contract_first(left, right):
    return lax.dot_general(
        left, right, (((0,), (0,)), ((), ())), preferred_element_type=jnp.float32
    )


def conv_ahead(extended, taps, bias, length):
    total = jnp.zeros((length, extended.shape[1]), jnp.float32) + bias.astype(jnp.float32)
    for offset in range(taps.shape[0]):
        total = total + taps[offset].astype(jnp.float32) * extended[offset : offset + length]
    return total


def conv_behind(extended, taps, length):
    reach = taps.shape[0] - 1
    total = jnp.zeros((length, extended.shape[1]), jnp.float32)
    for offset in range(taps.shape[0]):
        total = (
            total
            + taps[offset].astype(jnp.float32) * extended[reach - offset : reach - offset + length]
        )
    return total.astype(jnp.bfloat16)


def tap_grads(grad_pre, extended, tap_count):
    length = grad_pre.shape[0]
    rows = [
        jnp.sum(grad_pre * extended[offset : offset + length], axis=0)
        for offset in range(tap_count)
    ]
    return (jnp.stack(rows, 0), jnp.sum(grad_pre, axis=0))


def per_device(
    hidden_in,
    up_act,
    up_val,
    cotangent,
    w_act,
    w_val,
    w_down,
    conv_act,
    conv_val,
    bias_act,
    bias_val,
):
    local_rows = cotangent.shape[0]
    tap_count = conv_act.shape[0]
    reach = tap_count - 1
    tp_count = lax.axis_size("tp")
    fs_count = lax.axis_size("fs")
    down_whole = lax.all_gather(w_down, "tp", axis=1, tiled=True)
    prev_act, prev_val = passed_along(
        (up_act[local_rows - reach :], up_val[local_rows - reach :]), "tp", 1
    )
    ext_act = jnp.concatenate([prev_act, up_act], 0).astype(jnp.float32)
    ext_val = jnp.concatenate([prev_val, up_val], 0).astype(jnp.float32)
    pre_act = conv_ahead(ext_act, conv_act, bias_act, local_rows)
    pre_val = conv_ahead(ext_val, conv_val, bias_val, local_rows)
    gelu_act, gelu_back = jax.vjp(jax.nn.gelu, pre_act)
    mixed = (gelu_act * pre_val).astype(jnp.bfloat16)
    grad_mixed = contract_last(cotangent, down_whole).astype(jnp.bfloat16)
    grad_mixed = lax.optimization_barrier(grad_mixed).astype(jnp.float32)
    grad_pre_act = gelu_back(grad_mixed * pre_val)[0]
    grad_pre_val = grad_mixed * gelu_act
    next_act, next_val = passed_along((grad_pre_act[:reach], grad_pre_val[:reach]), "tp", -1)
    grad_up_act = conv_behind(jnp.concatenate([grad_pre_act, next_act], 0), conv_act, local_rows)
    grad_up_val = conv_behind(jnp.concatenate([grad_pre_val, next_val], 0), conv_val, local_rows)
    taps_act, sums_act = tap_grads(grad_pre_act, ext_act, tap_count)
    taps_val, sums_val = tap_grads(grad_pre_val, ext_val, tap_count)
    all_up_act, all_up_val, all_mixed = (
        lax.all_gather(grad_up_act, "tp", axis=0, tiled=True),
        lax.all_gather(grad_up_val, "tp", axis=0, tiled=True),
        lax.all_gather(mixed, "tp", axis=0, tiled=True),
    )
    cot_columns = lax.all_to_all(cotangent, "tp", split_axis=1, concat_axis=0, tiled=True)
    grad_w_act = contract_first(hidden_in, all_up_act)
    grad_w_val = contract_first(hidden_in, all_up_val)
    grad_w_down = contract_first(all_mixed, cot_columns)
    shard_rows = local_rows // fs_count
    block_rows = tp_count * shard_rows

    def select_rows(gathered):
        shaped = gathered.reshape(tp_count, fs_count, shard_rows, gathered.shape[1])
        return jnp.transpose(shaped, (1, 0, 2, 3)).reshape(
            lax.axis_size("fs") * block_rows, gathered.shape[1]
        )

    summed = lax.psum_scatter(
        contract_last(select_rows(all_up_act), w_act)
        + contract_last(select_rows(all_up_val), w_val),
        "fs",
        scatter_dimension=0,
        tiled=True,
    ).astype(jnp.bfloat16)
    grad_input = lax.all_to_all(summed, "tp", split_axis=0, concat_axis=1, tiled=True)
    down_squares = jnp.sum(grad_w_down * grad_w_down, axis=1)
    taps_act, taps_val, sums_act, sums_val, rows_down = lax.psum(
        (taps_act, taps_val, sums_act, sums_val, down_squares), "tp"
    )
    tap_squares = jnp.stack(
        [jnp.sum(taps_act * taps_act, axis=1), jnp.sum(taps_val * taps_val, axis=1)], 0
    )
    rows_act, rows_val, conv_rows = lax.psum(
        (
            jnp.sum(grad_w_act * grad_w_act, axis=1),
            jnp.sum(grad_w_val * grad_w_val, axis=1),
            tap_squares,
        ),
        "fs",
    )
    return (
        grad_input,
        grad_w_act,
        grad_w_val,
        grad_w_down,
        taps_act,
        taps_val,
        sums_act,
        sums_val,
        rows_act,
        rows_val,
        rows_down,
        conv_rows,
    )


def solution(mesh):
    return jax.shard_map(
        per_device,
        mesh=mesh,
        in_specs=(
            P(None, "tp"),
            P("tp", "fs"),
            P("tp", "fs"),
            P("tp", None),
            P("tp", "fs"),
            P("tp", "fs"),
            P("fs", "tp"),
            P(None, "fs"),
            P(None, "fs"),
            P("fs"),
            P("fs"),
        ),
        out_specs=(
            P(("tp", "fs"), None),
            P("tp", "fs"),
            P("tp", "fs"),
            P("fs", "tp"),
            P(None, "fs"),
            P(None, "fs"),
            P("fs"),
            P("fs"),
            P("tp"),
            P("tp"),
            P("fs"),
            P(),
        ),
        check_vma=False,
    )
```

profile of v0, /device:TPU:0, one launch (start us, length us, event | category | flops | bytes accessed | tf_op | source)
XLA Modules:
  0.0 296.1 jit_solution(9692622403794457745)
XLA Ops:
  7.2 0.7 all-gather.5.cloned.1.call-update
  8.0 0.4 copy-done.10
  8.4 2.4 collective-permute-start.1
  10.8 0.8 slice.74
  11.5 4.5 %collective-permute-start = (bf16[2,1536]{1,0:T(2,128)(2,1)S(1)}, bf16[2,1536]{1,0:T(2,128)(2,1)S(1)}, u32[]{:S(2)}, u32[]{:S(2)}) collective-permute-start(bf16[2,1536]{1,0:T(2,128)(2,1)S(1)} %slice.74), channel_id=1, source_target_pairs={{0,1},{1,2},{2,3},{4,5},{5,6},{6,7},{8,9},{9,10},{10,11},{12,13},{... | collective-permute-start | bytes 18440 | tf_op jit(solution)/shard_map/ppermute | solution.py:10
  16.0 1.5 convert_reduce_fusion.5
  17.5 1.3 convert_element_type.52
  18.8 1.0 maximum_convert_fusion.1
  19.8 2.1 maximum_convert_fusion
  21.9 72.5 %all-gather.5.cloned.1.call-done = bf16[1536,4096]{1,0:T(8,128)(2,1)} async-done(((bf16[1536,1024]{1,0:T(8,128)(2,1)}), bf16[1536,4096]{1,0:T(8,128)(2,1)}) %all-gather.5.cloned.1.call-update) | async-done | bytes 12582928 | tf_op jit(solution)/shard_map/all_gather | solution.py:70
  94.4 9.3 %convolution_convert_fusion = bf16[128,1536]{1,0:T(8,128)(2,1)S(1)} fusion(bf16[128,4096]{1,0:T(8,128)(2,1)} %param.14, bf16[1536,4096]{1,0:T(8,128)(2,1)} %all-gather.5.cloned.1.call-done), kind=kOutput, calls=%fused_computation.5 | convolution fusion | flops 1610809344 | bytes 14024704 | tf_op jit(solution)/shard_map/dot_general | solution.py:14
  103.8 0.9 multiply_reduce_fusion.5
  104.7 1.3 collective-permute-start.3
  106.0 0.1 convert_reduce_fusion.4
  106.1 1.7 collective-permute-done.3
  107.8 2.1 multiply_reduce_fusion.8
  110.0 0.8 slice.98
  110.8 1.3 collective-permute-start.2
  112.1 3.5 %collective-permute-done.2 = f32[2,1536]{1,0:T(2,128)S(1)} collective-permute-done((f32[2,1536]{1,0:T(2,128)S(1)}, f32[2,1536]{1,0:T(2,128)S(1)}, u32[]{:S(2)}, u32[]{:S(2)}) %collective-permute-start.2) | collective-permute-done | bytes 12320 | tf_op jit(solution)/shard_map/ppermute | solution.py:10
  115.5 3.0 fusion.9
  118.5 0.0 all-gather.11.cloned.1.call-start
  118.6 2.5 multiply_convert_fusion
  121.1 0.0 reduce-scatter.2.cloned.1.call-start
  121.2 10.4 %all-gather.9.cloned.1.call-done = bf16[512,1536]{1,0:T(8,128)(2,1)} async-done(((bf16[128,1536]{1,0:T(8,128)(2,1)}), bf16[512,1536]{1,0:T(8,128)(2,1)}) %all-gather.9.cloned.1.call-update) | async-done | bytes 1572880 | tf_op jit(solution)/shard_map/all_gather | solution.py:91
  131.5 2.7 copy.34
  134.2 18.6 %all-gather.7.cloned.1.call-done = bf16[512,1536]{1,0:T(8,128)(2,1)} async-done(((bf16[128,1536]{1,0:T(8,128)(2,1)}), bf16[512,1536]{1,0:T(8,128)(2,1)}) %all-gather.7.cloned.1.call-update) | async-done | bytes 1572880 | tf_op jit(solution)/shard_map/all_gather | solution.py:90
  152.8 1.5 copy.33
  154.3 1.8 fusion.19
  156.2 0.5 copy-done.17
  156.7 3.2 %convolution_add_fusion = f32[512,1024]{1,0:T(8,128)} fusion(f32[512,1024]{1,0:T(8,128)S(1)} %fusion.19, bf16[512,1536]{1,0:T(8,128)(2,1)S(1)} %bitcast.37, bf16[1024,1536]{1,0:T(8,128)(2,1)S(1)} %copy-done.17), kind=kOutput, calls=%fused_computation.6 | convolution fusion | flops 1611137024 | bytes 8912896 | tf_op jit(solution)/shard_map/dot_general | solution.py:14
  159.9 1.3 copy-done.5
  161.1 0.7 copy.36
  161.8 21.8 %all_to_all.38 = bf16[128,4,1024]{0,2,1:T(8,128)(2,1)S(1)} all-to-all(bf16[128,4,1024]{0,2,1:T(8,128)(2,1)S(1)} %bitcast.34), channel_id=1, replica_groups=mesh['fs'=8,'tp'=4] {'tp'}, dimensions={1} | all-to-all | bytes 2097152 | tf_op jit(solution)/shard_map/all_to_all | solution.py:94
  183.6 1.3 copy.37
  185.0 0.3 copy-done.7
  185.4 5.8 %multiply_reduce_fusion.1 = (f32[1024]{0:T(1024)S(1)}, f32[1024,1536]{0,1:T(8,128)}) fusion(bf16[512,1536]{1,0:T(8,128)(2,1)S(1)} %copy-done.7, bf16[512,1024]{1,0:T(8,128)(2,1)} %param.11), kind=kOutput, calls=%fused_computation.1 | convolution fusion | flops 1613757440 | bytes 8916992 | tf_op jit(solution)/shard_map/dot_general | solution.py:20
  191.1 6.7 %copy.39 = f32[1024,1536]{1,0:T(8,128)} copy(f32[1024,1536]{0,1:T(8,128)} %get-tuple-element.80) | data formatting | bytes 12582912
  197.8 6.0 %multiply_reduce_fusion = (f32[1536]{0:T(1024)S(1)}, f32[1536,1024]{0,1:T(8,128)}) fusion(bf16[512,1536]{1,0:T(8,128)(2,1)} %all-gather.11.cloned.1.call-done, bf16[512,1024]{1,0:T(8,128)(2,1)S(1)} %bitcast.39), kind=kOutput, calls=%fused_computation | convolution fusion | flops 1613756928 | bytes 8919040 | tf_op jit(solution)/shard_map/dot_general | solution.py:20
  203.8 6.7 %copy.40 = f32[1536,1024]{1,0:T(8,128)} copy(f32[1536,1024]{0,1:T(8,128)} %get-tuple-element.76) | data formatting | bytes 12582912
  210.5 11.9 %all-reduce.1 = (f32[3,1536]{1,0:T(4,128)S(1)}, f32[3,1536]{1,0:T(4,128)S(1)}, f32[1536]{0:T(1024)}, f32[1536]{0:T(1024)}, f32[1536]{0:T(1024)}) all-reduce(f32[3,1536]{1,0:T(4,128)S(1)} %pad_maximum_fusion.2, f32[3,1536]{1,0:T(4,128)S(1)} %pad_maximum_fusion.3, ...), channel_id=1, replica_groups=mesh['fs'=8,'tp'=4] {'tp'}, use_global_device_ids=true, to_apply=%region_4.0 | all-reduce | flops 13824 | bytes 110592 | tf_op jit(solution)/shard_map/psum | solution.py:116
  222.4 0.2 multiply_reduce_fusion.9
  222.6 28.7 %reduce-scatter.2.cloned.1.call-done = f32[64,1024]{1,0:T(8,128)} async-done(((f32[512,1024]{1,0:T(8,128)}), f32[64,1024]{1,0:T(8,128)}) %reduce-scatter.2.cloned.1.call-update) | async-done | bytes 262160 | tf_op jit(solution)/shard_map/reduce_scatter | solution.py:107
  251.3 1.6 convert_element_type.56
  252.9 3.3 %all-to-all-start = ((bf16[4,16,1024]{2,1,0:T(8,128)(2,1)}), bf16[4,16,1024]{2,1,0:T(8,128)(2,1)S(1)}, u32[]{:S(2)}, u32[]{:S(2)}) async-start(bf16[4,16,1024]{2,1,0:T(8,128)(2,1)} %bitcast.6), calls=%async_computation.1 | async-start | bytes 262144 | tf_op jit(solution)/shard_map/all_to_all | solution.py:114
  256.3 5.7 %multiply_reduce_fusion.2 = (f32[1024]{0:T(1024)S(1)}, f32[1024,1536]{0,1:T(8,128)}) fusion(bf16[512,1536]{1,0:T(8,128)(2,1)S(1)} %copy-done.6, bf16[512,1024]{1,0:T(8,128)(2,1)} %param.11), kind=kOutput, calls=%fused_computation.2 | convolution fusion | flops 1613757440 | bytes 8916992 | tf_op jit(solution)/shard_map/dot_general | solution.py:20
  262.0 6.7 %copy.38 = f32[1024,1536]{1,0:T(8,128)} copy(f32[1024,1536]{0,1:T(8,128)} %get-tuple-element.78) | data formatting | bytes 12582912
  268.7 20.2 %all-reduce = (f32[1024]{0:T(1024)}, f32[1024]{0:T(1024)}, f32[2,3]{1,0:T(2,128)}) all-reduce(f32[1024]{0:T(1024)S(1)} %get-tuple-element.77, f32[1024]{0:T(1024)S(1)} %get-tuple-element.79, f32[2,3]{1,0:T(2,128)S(1)} %pad_maximum_fusion.4), channel_id=1, replica_groups=mesh['fs'=8,'tp'=4] {'fs'}, use_global_device_ids=true, to_apply=%region_14.0 | all-reduce | flops 2054 | bytes 16432 | tf_op jit(solution)/shard_map/psum | solution.py:122
  288.9 0.7 copy.41
  (55 shorter events, 0.4 us)
Async XLA Ops:
  7.2 147.1 %copy-start = (bf16[1024,1536]{1,0:T(8,128)(2,1)S(1)}, bf16[1024,1536]{1,0:T(8,128)(2,1)}, u32[]{:S(2)}) copy-start(bf16[1024,1536]{1,0:T(8,128)(2,1)} %param.15) | copy-start | bytes 9437188
  7.2 1.1 copy-start.10
  7.2 87.2 %all-gather.5.cloned.1.call-start = ((), (), s32[]{:S(2)}) async-start(), calls=%async_computation.3 | async-start | bytes 15728640 | tf_op jit(solution)/shard_map/all_gather | solution.py:70
  7.9 123.6 %all-gather.9.cloned.1.call-start = ((), (), s32[]{:S(2)}) async-start(), calls=%async_computation.5 | async-start | bytes 1966080 | tf_op jit(solution)/shard_map/all_gather | solution.py:91
  8.4 10.4 %collective-permute-start.1 = (bf16[2,1536]{1,0:T(2,128)(2,1)S(1)}, bf16[2,1536]{1,0:T(2,128)(2,1)S(1)}, u32[]{:S(2)}, u32[]{:S(2)}) collective-permute-start(bf16[2,1536]{1,0:T(2,128)(2,1)S(1)} %slice.80), channel_id=1, source_target_pairs={{0,1},{1,2},{2,3},{4,5},{5,6},{6,7},{8,9},{9,10},{10,11},{12,13},{... | collective-permute-start | bytes 18440 | tf_op jit(solution)/shard_map/ppermute | solution.py:10
  11.5 8.3 %collective-permute-start = (bf16[2,1536]{1,0:T(2,128)(2,1)S(1)}, bf16[2,1536]{1,0:T(2,128)(2,1)S(1)}, u32[]{:S(2)}, u32[]{:S(2)}) collective-permute-start(bf16[2,1536]{1,0:T(2,128)(2,1)S(1)} %slice.74), channel_id=1, source_target_pairs={{0,1},{1,2},{2,3},{4,5},{5,6},{6,7},{8,9},{9,10},{10,11},{12,13},{... | collective-permute-start | bytes 18440 | tf_op jit(solution)/shard_map/ppermute | solution.py:10
  21.9 81.8 %copy-start.11 = (f32[1536]{0:T(1024)S(1)}, f32[1536]{0:T(1024)}, u32[]{:S(2)}) copy-start(f32[1536]{0:T(1024)} %get-tuple-element.61) | copy-start | bytes 18436
  21.9 81.8 %copy-start.12 = (f32[1536]{0:T(1024)S(1)}, f32[1536]{0:T(1024)}, u32[]{:S(2)}) copy-start(f32[1536]{0:T(1024)} %convert_element_type.52) | copy-start | bytes 18436
  94.4 9.3 %copy-start.2 = (f32[130,1536]{1,0:T(8,128)S(1)}, f32[130,1536]{1,0:T(8,128)}, u32[]{:S(2)}) copy-start(f32[130,1536]{1,0:T(8,128)} %maximum_convert_fusion.1) | copy-start | bytes 2396164
  94.4 9.3 %copy-start.3 = (f32[130,1536]{1,0:T(8,128)S(1)}, f32[130,1536]{1,0:T(8,128)}, u32[]{:S(2)}) copy-start(f32[130,1536]{1,0:T(8,128)} %maximum_convert_fusion) | copy-start | bytes 2396164
  103.8 2.2 copy-start.13
  103.8 2.3 copy-start.16
  104.7 5.2 %copy-start.4 = (f32[128,1536]{1,0:T(8,128)}, f32[128,1536]{1,0:T(8,128)S(1)}, u32[]{:S(2)}) copy-start(f32[128,1536]{1,0:T(8,128)S(1)} %get-tuple-element.71) | copy-start | bytes 2359300
  104.7 3.1 %collective-permute-start.3 = (f32[2,1536]{1,0:T(2,128)S(1)}, f32[2,1536]{1,0:T(2,128)S(1)}, u32[]{:S(2)}, u32[]{:S(2)}) collective-permute-start(f32[2,1536]{1,0:T(2,128)S(1)} %slice.101), channel_id=1, source_target_pairs={{1,0},{2,1},{3,2},{5,4},{6,5},{7,6},{9,8},{10,9},{11,10},{13,12},{... | collective-permute-start | bytes 36872 | tf_op jit(solution)/shard_map/ppermute | solution.py:10
  109.9 42.9 %all-gather.7.cloned.1.call-start = ((), (), s32[]{:S(2)}) async-start(), calls=%async_computation.4 | async-start | bytes 1966080 | tf_op jit(solution)/shard_map/all_gather | solution.py:90
  110.8 4.8 %collective-permute-start.2 = (f32[2,1536]{1,0:T(2,128)S(1)}, f32[2,1536]{1,0:T(2,128)S(1)}, u32[]{:S(2)}, u32[]{:S(2)}) collective-permute-start(f32[2,1536]{1,0:T(2,128)S(1)} %slice.98), channel_id=1, source_target_pairs={{1,0},{2,1},{3,2},{5,4},{6,5},{7,6},{9,8},{10,9},{11,10},{13,12},{... | collective-permute-start | bytes 36872 | tf_op jit(solution)/shard_map/ppermute | solution.py:10
  118.5 79.3 %all-gather.11.cloned.1.call-start = ((), (), s32[]{:S(2)}) async-start(), calls=%async_computation.7 | async-start | bytes 1966080 | tf_op jit(solution)/shard_map/all_gather | solution.py:92
  121.1 130.2 %reduce-scatter.2.cloned.1.call-start = ((), (), s32[]{:S(2)}) async-start(), calls=%async_computation.6 | async-start | bytes 2359296 | tf_op jit(solution)/shard_map/reduce_scatter | solution.py:107
  154.3 1.9 copy-start.8
  154.3 2.4 copy-start.17
  159.8 1.3 copy-start.5
  183.6 1.8 copy-start.7
  191.1 6.7 %copy-start.9 = (bf16[4,128,1024]{2,1,0:T(8,128)(2,1)S(1)}, bf16[4,128,1024]{2,1,0:T(8,128)(2,1)}, u32[]{:S(2)}) copy-start(bf16[4,128,1024]{2,1,0:T(8,128)(2,1)} %copy.37) | copy-start | bytes 3145732
  203.8 52.5 %copy-start.6 = (bf16[512,1536]{1,0:T(8,128)(2,1)S(1)}, bf16[512,1536]{1,0:T(8,128)(2,1)}, u32[]{:S(2)}) copy-start(bf16[512,1536]{1,0:T(8,128)(2,1)} %all-gather.7.cloned.1.call-done) | copy-start | bytes 4718596
  222.4 39.5 %copy-start.14 = (f32[3,1536]{1,0:T(4,128)}, f32[3,1536]{1,0:T(4,128)S(1)}, u32[]{:S(2)}) copy-start(f32[3,1536]{1,0:T(4,128)S(1)} %get-tuple-element.65) | copy-start | bytes 55300
  222.4 39.5 %copy-start.15 = (f32[3,1536]{1,0:T(4,128)}, f32[3,1536]{1,0:T(4,128)S(1)}, u32[]{:S(2)}) copy-start(f32[3,1536]{1,0:T(4,128)S(1)} %get-tuple-element.66) | copy-start | bytes 55300
  252.9 35.9 %all-to-all-start = ((bf16[4,16,1024]{2,1,0:T(8,128)(2,1)}), bf16[4,16,1024]{2,1,0:T(8,128)(2,1)S(1)}, u32[]{:S(2)}, u32[]{:S(2)}) async-start(bf16[4,16,1024]{2,1,0:T(8,128)(2,1)} %bitcast.6), calls=%async_computation.1 | async-start | bytes 262144 | tf_op jit(solution)/shard_map/all_to_all | solution.py:114
  262.0 27.5 %copy-start.1 = (bf16[1024,1536]{1,0:T(8,128)(2,1)S(1)}, bf16[1024,1536]{1,0:T(8,128)(2,1)}, u32[]{:S(2)}) copy-start(bf16[1024,1536]{1,0:T(8,128)(2,1)} %param.15) | copy-start | bytes 9437188
Sparse Core Ops, SparseCore 0:
  9.6 84.7 all-gather.4
  110.0 21.4 all-gather.8
  133.1 19.6 all-gather.6
  154.2 24.6 all-gather.10
  182.2 68.9 reduce-scatter.1
where the time goes:
time: 297 us; the launch traced here: 296 us
  waiting for transfers between devices  136 us (46%)
  blocking collectives  53.9 us (18%)
  matrix products  31.7 us (11%)
  local copies, waits for them, and re-layouts  31 us (10%)
  other arithmetic  16.2 us (5%)
  between operations  14.1 us (5%)
  starting transfers between devices  13 us (4%)
    all_gather x1, waiting for transfers between devices, per_device(): down_whole = lax.all_gather(w_down, 'tp', axis=1, tiled=True)  72.5 us
    reduce_scatter x1, waiting for transfers between devices, per_device(): lax.psum_scatter(contract_last(select_rows(all_up_act), w_act) + contract...  28.7 us
    unnamed x40, local copies, waits for them, and re-layouts  23.3 us
    all_to_all x1, blocking collectives, per_device(): lax.all_to_all(cotangent, 'tp', split_axis=1, concat_axis=0, tiled=True)  21.8 us
    psum x1, blocking collectives, per_device(): lax.psum((jnp.sum(grad_w_act * grad_w_act, axis=1), jnp.sum(grad_w_val *...  20.2 us
    all_gather x1, waiting for transfers between devices, per_device(): lax.all_gather(grad_up_act, 'tp', axis=0, tiled=True)  18.6 us
    dot_general x3, matrix products, contract_first(): lax.dot_general(left, right, (((0,), (0,)), ((), ())), preferred_element_...  17.5 us
    dot_general x3, matrix products, contract_last(): lax.dot_general(left, right, (((1,), (1,)), ((), ())), preferred_element_...  14.3 us
  transfers between devices with their start and end apart: 10, of which 6 were waited for; matrix products, arithmetic and copies ran while one was open for 21% of the time, Pallas kernels for 0%

commit v1 on v0

--- a/solution.py
+++ b/solution.py
@@ -1,7 +1,453 @@
 import jax
 import jax.numpy as jnp
 from jax import lax
+from jax.experimental import pallas as pl
+from jax.experimental.pallas import tpu as pltpu
 from jax.sharding import PartitionSpec as P
+
+MESH = pl.DeviceIdType.MESH
+F32 = jnp.float32
+BF16 = jnp.bfloat16
+CHUNK = 256
+HALO = 16
+TAIL = 8
+ROOT_TWO_OVER_PI = 0.7978845608028654
+CUBIC = 0.044715
+
+
+def remote(copy_at, source, target, send, receive, where):
+    return pltpu.make_async_remote_copy(
+        src_ref=source,
+        dst_ref=target,
+        send_sem=send.at[copy_at],
+        recv_sem=receive.at[copy_at],
+        device_id=where,
+        device_id_type=MESH,
+    )
+
+
+def greet(everyone):
+    barrier = pltpu.get_barrier_semaphore()
+    for where in everyone:
+        pl.semaphore_signal(barrier, inc=1, device_id=where, device_id_type=MESH)
+    pl.semaphore_wait(barrier, len(everyone))
+
+
+def gradient_kernel(
+    cot, down, up_a, up_v, taps_a, taps_v, bias_a, bias_v,
+    columns, all_a, all_v, all_m, sums,
+    own, to_sib, to_sib_far, to_far, from_sib, from_sib_far, from_far,
+    before_a, before_v, grad_a, grad_v, after_a, after_v, own_sums, got_sums,
+    send, receive,
+):
+    me = lax.axis_index("tp")
+    count = lax.axis_size("tp")
+    chip, core = me // 2, me % 2
+    sib = chip * 2 + (1 - core)
+    far = (1 - chip) * 2 + core
+    diag = (1 - chip) * 2 + (1 - core)
+    right, left = lax.rem(me + 1, count), lax.rem(me + count - 1, count)
+    length, width = up_a.shape
+    depth = down.shape[1]
+    tap_count = taps_a.shape[0]
+    reach = tap_count - 1
+
+    def to(index):
+        return {"tp": index}
+
+    def rows(ref, index):
+        return ref.at[pl.ds(pl.multiple_of(index * length, length), length), :]
+
+    def cols(index):
+        return pl.ds(pl.multiple_of(index * depth, depth), depth)
+
+    greet([to(sib), to(far), to(diag)])
+    cot_copies = [
+        remote(slot, cot.at[:, cols(peer)], rows(columns, me), send, receive, to(peer))
+        for slot, peer in ((0, sib), (1, far), (2, diag))
+    ]
+    last = pl.ds(length - HALO, HALO)
+    halo_copies = [
+        remote(3, up_a.at[last, :], before_a, send, receive, to(right)),
+        remote(4, up_v.at[last, :], before_v, send, receive, to(right)),
+    ]
+    for copy in (cot_copies[1], cot_copies[2], cot_copies[0], *halo_copies):
+        copy.start()
+    rows(columns, me)[...] = cot[:, cols(me)]
+
+    def partial(index, finish):
+        block = rows(columns, index)[...]
+
+        def step(at, carry):
+            lanes = pl.ds(pl.multiple_of(at * CHUNK, CHUNK), CHUNK)
+            finish(lanes, contract_last(block, down[lanes, :]))
+            return carry
+
+        lax.fori_loop(0, width // CHUNK, step, 0)
+
+    def keep(target):
+        def finish(lanes, value):
+            target[:, lanes] = value.astype(target.dtype)
+
+        return finish
+
+    def add_far(lanes, value):
+        to_far[:, lanes] = (value + from_sib_far[:, lanes].astype(F32)).astype(BF16)
+
+    partial(me, keep(own))
+    cot_copies[0].wait_recv()
+    partial(sib, keep(to_sib))
+    near_copy = remote(5, to_sib, from_sib, send, receive, to(sib))
+    near_copy.start()
+    cot_copies[2].wait_recv()
+    partial(diag, keep(to_sib_far))
+    relay_copy = remote(6, to_sib_far, from_sib_far, send, receive, to(sib))
+    relay_copy.start()
+    cot_copies[1].wait_recv()
+    relay_copy.wait_recv()
+    partial(far, add_far)
+    far_copy = remote(7, to_far, from_far, send, receive, to(far))
+    far_copy.start()
+    for copy in halo_copies:
+        copy.wait_recv()
+    near_copy.wait_recv()
+    far_copy.wait_recv()
+
+    has_before = (me > 0).astype(F32)
+    has_after = (me < count - 1).astype(F32)
+    out_m, out_a, out_v = rows(all_m, me), rows(all_a, me), rows(all_v, me)
+
+    def forward(at, carry):
+        lanes = pl.ds(pl.multiple_of(at * CHUNK, CHUNK), CHUNK)
+        ext_a = jnp.concatenate(
+            [before_a[:, lanes].astype(F32) * has_before, up_a[:, lanes].astype(F32)], 0
+        )
+        ext_v = jnp.concatenate(
+            [before_v[:, lanes].astype(F32) * has_before, up_v[:, lanes].astype(F32)], 0
+        )
+        taken_a = [ext_a[HALO - reach + k : HALO - reach + k + length] for k in range(tap_count)]
+        taken_v = [ext_v[HALO - reach + k : HALO - reach + k + length] for k in range(tap_count)]
+        pre_a = jnp.broadcast_to(bias_a[:, lanes].astype(F32), (length, CHUNK))
+        pre_v = jnp.broadcast_to(bias_v[:, lanes].astype(F32), (length, CHUNK))
+        for k in range(tap_count):
+            pre_a = pre_a + taps_a[k : k + 1, lanes].astype(F32) * taken_a[k]
+            pre_v = pre_v + taps_v[k : k + 1, lanes].astype(F32) * taken_v[k]
+        square = pre_a * pre_a
+        bent = jnp.tanh(ROOT_TWO_OVER_PI * pre_a * (1.0 + CUBIC * square))
+        half = 0.5 * (1.0 + bent)
+        gelu = pre_a * half
+        slope = half + 0.5 * pre_a * (1.0 - bent * bent) * (
+            ROOT_TWO_OVER_PI * (1.0 + 3.0 * CUBIC * square)
+        )
+        out_m[:, lanes] = (gelu * pre_v).astype(BF16)
+        total = own[:, lanes] + from_sib[:, lanes].astype(F32) + from_far[:, lanes].astype(F32)
+        grad_mixed = total.astype(BF16).astype(F32)
+        pre_grad_a = grad_mixed * pre_v * slope
+        pre_grad_v = grad_mixed * gelu
+        grad_a[:, lanes] = pre_grad_a
+        grad_v[:, lanes] = pre_grad_v
+        found = [jnp.sum(pre_grad_a * taken, axis=0, keepdims=True) for taken in taken_a]
+        found.append(jnp.sum(pre_grad_a, axis=0, keepdims=True))
+        found += [jnp.sum(pre_grad_v * taken, axis=0, keepdims=True) for taken in taken_v]
+        found.append(jnp.sum(pre_grad_v, axis=0, keepdims=True))
+        own_sums[:, lanes] = jnp.concatenate(found, 0)
+        return carry
+
+    lax.fori_loop(0, width // CHUNK, forward, 0)
+    first = pl.ds(0, TAIL)
+    back_copies = [
+        remote(8, grad_a.at[first, :], after_a, send, receive, to(left)),
+        remote(9, grad_v.at[first, :], after_v, send, receive, to(left)),
+    ]
+    sum_copies = [
+        remote(19 + slot, own_sums, got_sums.at[slot], send, receive, to(peer))
+        for slot, peer in enumerate((sib, far, diag))
+    ]
+
+    def spread(slot, ref):
+        pair = [
+            remote(10 + slot, rows(ref, me), rows(ref, me), send, receive, to(far)),
+            remote(13 + slot, rows(ref, me), rows(ref, me), send, receive, to(sib)),
+        ]
+        for copy in pair:
+            copy.start()
+        return pair
+
+    for copy in back_copies:
+        copy.start()
+    spreads = [spread(0, all_m)]
+    for copy in sum_copies:
+        copy.start()
+
+    def backward(grads, after, taps, out):
+        def step(at, carry):
+            lanes = pl.ds(pl.multiple_of(at * CHUNK, CHUNK), CHUNK)
+            ext = jnp.concatenate([grads[:, lanes], after[:, lanes] * has_after], 0)
+            total = jnp.zeros((length, CHUNK), F32)
+            for k in range(tap_count):
+                total = total + taps[k : k + 1, lanes].astype(F32) * ext[reach - k : reach - k + length]
+            out[:, lanes] = total.astype(BF16)
+            return carry
+
+        lax.fori_loop(0, width // CHUNK, step, 0)
+
+    back_copies[0].wait_recv()
+    backward(grad_a, after_a, taps_a, out_a)
+    spreads.append(spread(1, all_a))
+    back_copies[1].wait_recv()
+    backward(grad_v, after_v, taps_v, out_v)
+    spreads.append(spread(2, all_v))
+    relays = []
+    for slot, (pair, ref) in enumerate(zip(spreads, (all_m, all_a, all_v))):
+        pair[0].wait_recv()
+        relay = remote(16 + slot, rows(ref, far), rows(ref, far), send, receive, to(sib))
+        relay.start()
+        relays.append(relay)
+    for copy in sum_copies:
+        copy.wait_recv()
+    sums[...] = (own_sums[...] + got_sums[0]) + (got_sums[1] + got_sums[2])
+    for pair, relay in zip(spreads, relays):
+        pair[1].wait_recv()
+        relay.wait_recv()
+    for copy in (
+        *cot_copies, *halo_copies, near_copy, relay_copy, far_copy, *back_copies, *sum_copies,
+        *(copy for pair in spreads for copy in pair), *relays,
+    ):
+        copy.wait_send()
+
+
+def gradients(cotangent, w_down, up_act, up_val, conv_act, conv_val, bias_act, bias_val):
+    length, width = up_act.shape
+    depth = w_down.shape[1]
+    tp_count = lax.axis_size("tp")
+    tap_count = conv_act.shape[0]
+    positions = length * tp_count
+    stat_rows = 2 * (tap_count + 1)
+    vmem = pl.BlockSpec(memory_space=pltpu.VMEM)
+    block = pltpu.VMEM((length, width), BF16)
+    wide = pltpu.VMEM((length, width), F32)
+    return pl.pallas_call(
+        gradient_kernel,
+        out_shape=(
+            jax.ShapeDtypeStruct((positions, depth), BF16),
+            jax.ShapeDtypeStruct((positions, width), BF16),
+            jax.ShapeDtypeStruct((positions, width), BF16),
+            jax.ShapeDtypeStruct((positions, width), BF16),
+            jax.ShapeDtypeStruct((stat_rows, width), F32),
+        ),
+        in_specs=[vmem] * 8,
+        out_specs=(vmem,) * 5,
+        scratch_shapes=[
+            wide, block, block, block, block, block, block,
+            pltpu.VMEM((HALO, width), BF16), pltpu.VMEM((HALO, width), BF16),
+            wide, wide,
+            pltpu.VMEM((TAIL, width), F32), pltpu.VMEM((TAIL, width), F32),
+            pltpu.VMEM((stat_rows, width), F32), pltpu.VMEM((3, stat_rows, width), F32),
+            pltpu.SemaphoreType.DMA((22,)), pltpu.SemaphoreType.DMA((22,)),
+        ],
+        compiler_params=pltpu.CompilerParams(
+            collective_id=0, has_side_effects=True, vmem_limit_bytes=50 * 1024 * 1024
+        ),
+    )(
+        cotangent, w_down, up_act, up_val, conv_act, conv_val,
+        bias_act.reshape(1, width), bias_val.reshape(1, width),
+    )
+
+
+def reduce_kernel(
+    terms, stat, down_stat, out, stat_sum, down_sum,
+    to_pair, from_pair, to_line, from_line, settled, got_stat, got_down,
+    send, receive,
+):
+    fs, tp = lax.axis_index("fs"), lax.axis_index("tp")
+    fs_count, tp_count = lax.axis_size("fs"), lax.axis_size("tp")
+    line = fs_count // 2
+    z, y = fs // 2, fs % 2
+    pair = z * 2 + (1 - y)
+    shard = out.shape[0]
+    depth = terms.shape[1]
+    length = terms.shape[0] // tp_count
+
+    def at_fs(index):
+        return {"fs": index}
+
+    def at_tp(index):
+        return {"tp": index}
+
+    fs_others = [lax.rem(fs + by, fs_count) for by in range(1, fs_count)]
+    tp_others = [lax.rem(tp + by, tp_count) for by in range(1, tp_count)]
+    greet([at_fs(i) for i in fs_others] + [at_tp(i) for i in tp_others])
+
+    def term(index):
+        return jnp.concatenate(
+            [
+                terms[pl.ds(pl.multiple_of(part * length + index * shard, shard), shard), :]
+                for part in range(tp_count)
+            ],
+            0,
+        )
+
+    base = 0
+    steps = sorted(range(1, line), key=lambda by: -min(by, line - by)) + [0]
+    there = {by: lax.rem(z + by, line) for by in steps}
+    pair_copies = {}
+    for by in steps:
+        to_pair[by] = term(there[by] * 2 + (1 - y)).astype(BF16)
+        pair_copies[by] = remote(
+            base + by, to_pair.at[by], from_pair.at[by], send, receive, at_fs(pair)
+        )
+        pair_copies[by].start()
+    base += line
+    small = []
+    for slot, index in enumerate(fs_others):
+        small.append(remote(base + slot, stat, got_stat.at[slot], send, receive, at_fs(index)))
+    base += len(fs_others)
+    for slot, index in enumerate(tp_others):
+        small.append(
+            remote(base + slot, down_stat, got_down.at[slot], send, receive, at_tp(index))
+        )
+    base += len(tp_others)
+    for copy in small:
+        copy.start()
+    line_copies = []
+    total = None
+    for by in steps:
+        pair_copies[by].wait_recv()
+        added = term(there[by] * 2 + y) + from_pair[by].astype(F32)
+        if by == 0:
+            total = added
+        else:
+            to_line[by] = added.astype(BF16)
+            copy = remote(
+                base + by, to_line.at[by], from_line.at[by], send, receive,
+                at_fs(there[by] * 2 + y),
+            )
+            copy.start()
+            line_copies.append((by, copy))
+    base += line
+    for by, copy in line_copies:
+        copy.wait_recv()
+        total = total + from_line[by].astype(F32)
+    settled[...] = total.astype(BF16)
+
+    def part_of(index):
+        return pl.ds(pl.multiple_of(index * shard, shard), shard)
+
+    mine = pl.ds(pl.multiple_of(tp * depth, depth), depth)
+    last_copies = [
+        remote(
+            base + slot, settled.at[part_of(index), :], out.at[:, mine], send, receive, at_tp(index)
+        )
+        for slot, index in enumerate(tp_others)
+    ]
+    for copy in last_copies:
+        copy.start()
+    out[:, mine] = settled[part_of(tp), :]
+    for copy in small:
+        copy.wait_recv()
+    stat_total = stat[...]
+    for slot in range(len(fs_others)):
+        stat_total = stat_total + got_stat[slot]
+    stat_sum[...] = stat_total
+    down_total = down_stat[...]
+    for slot in range(len(tp_others)):
+        down_total = down_total + got_down[slot]
+    down_sum[...] = down_total
+    for copy in last_copies:
+        copy.wait_recv()
+    for copy in (
+        *pair_copies.values(), *small, *(copy for _, copy in line_copies), *last_copies,
+    ):
+        copy.wait_send()
+
+
+def reduced(terms, stat, down_stat):
+    fs_count, tp_count = lax.axis_size("fs"), lax.axis_size("tp")
+    positions, depth = terms.shape
+    shard = positions // (fs_count * tp_count)
+    line = fs_count // 2
+    vmem = pl.BlockSpec(memory_space=pltpu.VMEM)
+    blocks = pltpu.VMEM((line, tp_count * shard, depth), BF16)
+    copies = 2 * line + (fs_count - 1) + 2 * (tp_count - 1)
+    return pl.pallas_call(
+        reduce_kernel,
+        out_shape=(
+            jax.ShapeDtypeStruct((shard, depth * tp_count), BF16),
+            jax.ShapeDtypeStruct(stat.shape, F32),
+            jax.ShapeDtypeStruct(down_stat.shape, F32),
+        ),
+        in_specs=[vmem] * 3,
+        out_specs=(vmem,) * 3,
+        scratch_shapes=[
+            blocks, blocks, blocks, blocks,
+            pltpu.VMEM((tp_count * shard, depth), BF16),
+            pltpu.VMEM((fs_count - 1,) + stat.shape, F32),
+            pltpu.VMEM((tp_count - 1,) + down_stat.shape, F32),
+            pltpu.SemaphoreType.DMA((copies,)), pltpu.SemaphoreType.DMA((copies,)),
+        ],
+        compiler_params=pltpu.CompilerParams(collective_id=1, has_side_effects=True),
+    )(terms, stat, down_stat)
+
+
+def kernels_fit(up_act, w_down, conv_act):
+    length, width = up_act.shape
+    fs_count, tp_count = lax.axis_size("fs"), lax.axis_size("tp")
+    return (
+        tp_count == 4
+        and fs_count % 2 == 0
+        and width % CHUNK == 0
+        and w_down.shape[1] % 128 == 0
+        and length % (16 * fs_count) == 0
+        and conv_act.shape[0] - 1 <= TAIL
+        and conv_act.shape[0] == 3
+        and width * (w_down.shape[1] + 24 * length) * 2 <= 24 * 1024 * 1024
+    )
+
+
+def with_kernels(
+    hidden_in, up_act, up_val, cotangent, w_act, w_val, w_down,
+    conv_act, conv_val, bias_act, bias_val,
+):
+    tap_count = conv_act.shape[0]
+    cot_columns, all_up_act, all_up_val, all_mixed, sums = gradients(
+        cotangent, w_down, up_act, up_val, conv_act, conv_val, bias_act, bias_val
+    )
+    grad_w_act = contract_first(hidden_in, all_up_act)
+    grad_w_val = contract_first(hidden_in, all_up_val)
+    grad_w_down = contract_first(all_mixed, cot_columns)
+    terms = contract_last(all_up_act, w_act) + contract_last(all_up_val, w_val)
+    taps_act, sums_act = sums[:tap_count], sums[tap_count]
+    taps_val, sums_val = sums[tap_count + 1 : 2 * tap_count + 1], sums[2 * tap_count + 1]
+    tap_squares = jnp.stack(
+        [jnp.sum(taps_act * taps_act, axis=1), jnp.sum(taps_val * taps_val, axis=1)], 0
+    )
+    depth = hidden_in.shape[1]
+    flat = tap_squares.reshape(1, -1)
+    stat = jnp.concatenate(
+        [
+            jnp.sum(grad_w_act * grad_w_act, axis=1)[None],
+            jnp.sum(grad_w_val * grad_w_val, axis=1)[None],
+            jnp.pad(flat, ((0, 0), (0, depth - flat.shape[1]))),
+            jnp.zeros((5, depth), F32),
+        ],
+        0,
+    )
+    down_stat = jnp.pad(jnp.sum(grad_w_down * grad_w_down, axis=1)[None], ((0, 7), (0, 0)))
+    grad_input, stat, down_stat = reduced(terms, stat, down_stat)
+    return (
+        grad_input,
+        grad_w_act,
+        grad_w_val,
+        grad_w_down,
+        taps_act,
+        taps_val,
+        sums_act,
+        sums_val,
+        stat[0],
+        stat[1],
+        down_stat[0],
+        stat[2, : 2 * tap_count].reshape(2, tap_count),
+    )
 
 
 def passed_along(value, axis, by):
@@ -62,6 +508,11 @@
     bias_act,
     bias_val,
 ):
+    if kernels_fit(up_act, w_down, conv_act):
+        return with_kernels(
+            hidden_in, up_act, up_val, cotangent, w_act, w_val, w_down,
+            conv_act, conv_val, bias_act, bias_val,
+        )
     local_rows = cotangent.shape[0]
     tap_count = conv_act.shape[0]
     reach = tap_count - 1

time: 297 us -> 153 us (0.52)
  waiting for transfers between devices: 136 us -> 0 us
  Pallas kernels: 0 us -> 97.3 us
  blocking collectives: 53.9 us -> 0 us
  other arithmetic: 16.2 us -> 1.45 us
  between operations: 14.1 us -> 0.74 us
  starting transfers between devices: 13 us -> 0 us
  matrix products: 31.7 us -> 20.1 us
    all_gather x4 -> x0, waiting for transfers between devices: 101 us -> none  [the longest x1 72.5 us: per_device(): down_whole = lax.all_gather(w_down, 'tp', axis=1, tiled=True)]
    pallas_call x0 -> x2, Pallas kernels: none -> 97.3 us  [the longest x1 69.2 us: gradients(): pl.pallas_call(gradient_kernel, out_shape=(jax.ShapeDtypeStruct((position...]
    psum x2 -> x0, blocking collectives: 32.1 us -> none  [the longest x1 20.2 us: per_device(): lax.psum((jnp.sum(grad_w_act * grad_w_act, axis=1), jnp.sum(grad_w_val *...]
    reduce_scatter x1 -> x0, waiting for transfers between devices: 28.7 us -> none  [per_device(): lax.psum_scatter(contract_last(select_rows(all_up_act), w_act) + contract...]
    all_to_all x1 -> x0, blocking collectives: 21.8 us -> none  [per_device(): lax.all_to_all(cotangent, 'tp', split_axis=1, concat_axis=0, tiled=True)]
    convert_element_type x7 -> x0, other arithmetic: 11.5 us -> none  [the longest x1 2.96 us: conv_behind(): return total.astype(jnp.bfloat16)]
    ppermute x4 -> x0, starting transfers between devices: 9.47 us -> none  [passed_along(): return lax.ppermute(value, axis, pairs)]
    dot_general x3 -> x2, matrix products: 14.3 us -> 6.52 us  [contract_last(): lax.dot_general(left, right, (((1,), (1,)), ((), ())), preferred_element_...]
  transfers between devices with their start and end apart: 10 -> 0, of which waited for: 6 -> 0; matrix products, arithmetic and copies ran while one was open for 21% -> 0% of each run, Pallas kernels for 0% -> 0%
where the time goes in v1:
time: 153 us; the launch traced here: 152 us
  Pallas kernels  97.3 us (64%)
  local copies, waits for them, and re-layouts  32.6 us (21%)
  matrix products  20.1 us (13%)
    pallas_call x1, Pallas kernels, gradients(): pl.pallas_call(gradient_kernel, out_shape=(jax.ShapeDtypeStruct((position...  69.2 us
    pallas_call x1, Pallas kernels, reduced(): pl.pallas_call(reduce_kernel, out_shape=(jax.ShapeDtypeStruct((shard, dep...  28.1 us
    unnamed x32, local copies, waits for them, and re-layouts  26 us
    dot_general x3, matrix products, contract_first(): lax.dot_general(left, right, (((0,), (0,)), ((), ())), preferred_element_...  13.6 us
    dot_general x2, matrix products, contract_last(): lax.dot_general(left, right, (((1,), (1,)), ((), ())), preferred_element_...  6.52 us

profile of v1, /device:TPU:0, one launch (start us, length us, event | category | flops | bytes accessed | tf_op | source)
XLA Modules:
  0.0 152.2 jit_solution(9974993454508786187)
XLA Ops:
  0.6 0.0 copy-start
  0.7 0.1 pad.13.clone
  0.7 0.8 reshape.33.bias_a
  1.6 0.7 reshape.34.bias_v
  2.3 0.0 copy-start.1
  2.3 1.2 copy-done.1
  3.5 0.0 copy-start.2
  3.5 1.0 copy-done.2
  4.5 0.0 copy-start.3
  4.5 1.0 copy-done.3
  5.5 0.0 copy-start.4
  5.5 0.7 copy-done.4
  6.2 0.0 copy-start.5
  6.2 0.7 copy-done.5
  6.9 69.2 %shard_map.202 = (bf16[512,1024]{1,0:T(8,128)(2,1)S(1)}, bf16[512,1536]{1,0:T(8,128)(2,1)}, bf16[512,1536]{1,0:T(8,128)(2,1)}, bf16[512,1536]{1,0:T(8,128)(2,1)}, f32[8,1536]{1,0:T(8,128)S(1)}) custom-call(bf16[128,4096]{1,0:T(8,128)(2,1)S(1)} %copy-done.1, bf16[1536,1024]{1,0:T(8,128)(2,1)} %down.1, bf16[128,1536]{1,0:T(8,128)(2,1)S(1)} %copy-done.2, ...), custom_call_target="tpu_custom_call" | custom-call | tf_op jit(solution)/shard_map/pallas_call | solution.py:229
  76.1 0.0 copy-start.6
  76.1 1.0 copy-done.6
  77.1 0.8 multiply_reduce_fusion.4
  77.9 0.1 reshape.35
  78.0 0.0 copy-done
  78.0 0.0 copy-start.9
  78.0 0.0 copy-start.11
  78.0 3.4 %fusion.3 = f32[512,1024]{1,0:T(8,128)S(1)} fusion(bf16[512,1536]{1,0:T(8,128)(2,1)} %get-tuple-element.20, bf16[1024,1536]{1,0:T(8,128)(2,1)S(1)} %copy-done), kind=kOutput, calls=%fused_computation.19 | convolution fusion | flops 1610612736 | bytes 6815744 | tf_op jit(solution)/shard_map/dot_general | solution.py:460
  81.4 0.0 copy-done.9
  81.4 0.0 copy-done.11
  81.4 0.0 copy-start.7
  81.4 0.0 copy-start.12
  81.4 3.1 %convolution_add_fusion.terms = f32[512,1024]{1,0:T(8,128)} fusion(f32[512,1024]{1,0:T(8,128)S(1)} %fusion.3, bf16[512,1536]{1,0:T(8,128)(2,1)S(1)} %copy-done.11, bf16[1024,1536]{1,0:T(8,128)(2,1)S(1)} %copy-done.9), kind=kOutput, calls=%fused_computation.5 | convolution fusion | flops 1611137024 | bytes 8912896 | tf_op jit(solution)/shard_map/dot_general | solution.py:460
  84.5 0.0 copy-done.7
  84.5 0.0 copy-done.12
  84.5 0.0 copy-start.13
  84.5 4.5 %multiply_reduce_fusion = (f32[1536]{0:T(1024)S(1)}, f32[1536,1024]{0,1:T(8,128)}) fusion(bf16[512,1536]{1,0:T(8,128)(2,1)S(1)} %copy-done.12, bf16[512,1024]{1,0:T(8,128)(2,1)S(1)} %copy-done.7), kind=kOutput, calls=%fused_computation | convolution fusion | flops 1613756928 | bytes 8919040 | tf_op jit(solution)/shard_map/dot_general | solution.py:466
  89.1 0.6 pad.9.down_stat
  89.7 0.0 copy-done.13
  89.7 4.6 %multiply_reduce_fusion.1 = (f32[1024]{0:T(1024)S(1)}, f32[1024,1536]{0,1:T(8,128)}) fusion(bf16[512,1536]{1,0:T(8,128)(2,1)S(1)} %copy-done.11, bf16[512,1024]{1,0:T(8,128)(2,1)S(1)} %copy-done.13), kind=kOutput, calls=%fused_computation.1 | convolution fusion | flops 1613757440 | bytes 8916992 | tf_op jit(solution)/shard_map/dot_general | solution.py:466
  94.2 0.0 copy-done.10
  94.2 4.5 %multiply_reduce_fusion.2 = (f32[1024]{0:T(1024)S(1)}, f32[1024,1536]{0,1:T(8,128)}) fusion(bf16[512,1536]{1,0:T(8,128)(2,1)S(1)} %copy-done.10, bf16[512,1024]{1,0:T(8,128)(2,1)S(1)} %copy-done.13), kind=kOutput, calls=%fused_computation.2 | convolution fusion | flops 1613757440 | bytes 8916992 | tf_op jit(solution)/shard_map/dot_general | solution.py:466
  98.8 0.7 fusion.stat
  99.5 28.1 %shard_map.203 = (bf16[16,4096]{1,0:T(8,128)(2,1)}, f32[8,1024]{1,0:T(8,128)}, f32[8,1536]{1,0:T(8,128)}) custom-call(f32[512,1024]{1,0:T(8,128)} %convolution_add_fusion.terms, f32[8,1024]{1,0:T(8,128)} %fusion.stat, f32[8,1536]{1,0:T(8,128)} %pad.9.down_stat), custom_call_target="tpu_custom_call" | custom-call | tf_op jit(solution)/shard_map/pallas_call | solution.py:372
  127.6 1.5 slice_reduce_fusion.1
  129.1 0.7 slice_reduce_fusion.3
  129.8 1.4 fusion.2
  131.2 0.6 reshape_squeeze.3
  131.9 6.6 %copy.23 = f32[1024,1536]{1,0:T(8,128)} copy(f32[1024,1536]{0,1:T(8,128)} %get-tuple-element.53) | data formatting | bytes 12582912
  138.4 6.6 %copy.24 = f32[1024,1536]{1,0:T(8,128)} copy(f32[1024,1536]{0,1:T(8,128)} %get-tuple-element.51) | data formatting | bytes 12582912
  145.0 6.6 %copy.25 = f32[1536,1024]{1,0:T(8,128)} copy(f32[1536,1024]{0,1:T(8,128)} %get-tuple-element.55) | data formatting | bytes 12582912
  151.6 0.0 copy-done.8
  151.6 0.7 copy.27
  (5 shorter events, 0.0 us)
Async XLA Ops:
  0.6 77.3 %copy-start = (bf16[1024,1536]{1,0:T(8,128)(2,1)S(1)}, bf16[1024,1536]{1,0:T(8,128)(2,1)}, u32[]{:S(2)}) copy-start(bf16[1024,1536]{1,0:T(8,128)(2,1)} %param.15) | copy-start | bytes 9437188
  2.3 1.2 copy-start.1
  3.5 1.0 copy-start.2
  4.5 1.0 copy-start.3
  5.5 0.7 copy-start.4
  6.2 0.7 copy-start.5
  76.1 1.0 copy-start.6
  78.0 3.4 %copy-start.9 = (bf16[1024,1536]{1,0:T(8,128)(2,1)S(1)}, bf16[1024,1536]{1,0:T(8,128)(2,1)}, u32[]{:S(2)}) copy-start(bf16[1024,1536]{1,0:T(8,128)(2,1)} %param.16) | copy-start | bytes 9437188
  78.0 3.4 %copy-start.11 = (bf16[512,1536]{1,0:T(8,128)(2,1)S(1)}, bf16[512,1536]{1,0:T(8,128)(2,1)}, u32[]{:S(2)}) copy-start(bf16[512,1536]{1,0:T(8,128)(2,1)} %get-tuple-element.21) | copy-start | bytes 4718596
  81.4 3.2 %copy-start.7 = (bf16[512,1024]{1,0:T(8,128)(2,1)S(1)}, bf16[512,1024]{1,0:T(8,128)(2,1)}, u32[]{:S(2)}) copy-start(bf16[512,1024]{1,0:T(8,128)(2,1)} %copy-done.6) | copy-start | bytes 3145732
  81.4 3.2 %copy-start.12 = (bf16[512,1536]{1,0:T(8,128)(2,1)S(1)}, bf16[512,1536]{1,0:T(8,128)(2,1)}, u32[]{:S(2)}) copy-start(bf16[512,1536]{1,0:T(8,128)(2,1)} %get-tuple-element.23) | copy-start | bytes 4718596
  84.5 5.1 %copy-start.13 = (bf16[512,1024]{1,0:T(8,128)(2,1)S(1)}, bf16[512,1024]{1,0:T(8,128)(2,1)}, u32[]{:S(2)}) copy-start(bf16[512,1024]{1,0:T(8,128)(2,1)} %param.11) | copy-start | bytes 3145732
  89.7 4.6 %copy-start.10 = (bf16[512,1536]{1,0:T(8,128)(2,1)S(1)}, bf16[512,1536]{1,0:T(8,128)(2,1)}, u32[]{:S(2)}) copy-start(bf16[512,1536]{1,0:T(8,128)(2,1)} %get-tuple-element.20) | copy-start | bytes 4718596
  145.0 6.6 %copy-start.8 = (bf16[16,4096]{1,0:T(8,128)(2,1)S(1)}, bf16[16,4096]{1,0:T(8,128)(2,1)}, u32[]{:S(2)}) copy-start(bf16[16,4096]{1,0:T(8,128)(2,1)} %get-tuple-element.69) | copy-start | bytes 393220

commit v2 on v1

--- a/solution.py
+++ b/solution.py
@@ -34,11 +34,12 @@
 
 
 def gradient_kernel(
-    cot, down, up_a, up_v, taps_a, taps_v, bias_a, bias_v,
-    columns, all_a, all_v, all_m, sums,
+    cot, down, up_a, up_v, taps_a, taps_v, bias_a, bias_v, weights_a, weights_v,
+    columns, all_a, all_v, all_m, sums, terms,
     own, to_sib, to_sib_far, to_far, from_sib, from_sib_far, from_far,
     before_a, before_v, grad_a, grad_v, after_a, after_v, own_sums, got_sums,
-    send, receive,
+    gated, factor, held_a, held_v,
+    send, receive, loaded,
 ):
     me = lax.axis_index("tp")
     count = lax.axis_size("tp")
@@ -61,6 +62,12 @@
     def cols(index):
         return pl.ds(pl.multiple_of(index * depth, depth), depth)
 
+    loads = [
+        pltpu.make_async_copy(weights_a, held_a, loaded.at[0]),
+        pltpu.make_async_copy(weights_v, held_v, loaded.at[1]),
+    ]
+    for load in loads:
+        load.start()
     greet([to(sib), to(far), to(diag)])
     cot_copies = [
         remote(slot, cot.at[:, cols(peer)], rows(columns, me), send, receive, to(peer))
@@ -94,7 +101,50 @@
     def add_far(lanes, value):
         to_far[:, lanes] = (value + from_sib_far[:, lanes].astype(F32)).astype(BF16)
 
+    has_before = (me > 0).astype(F32)
+    has_after = (me < count - 1).astype(F32)
+    out_m, out_a, out_v = rows(all_m, me), rows(all_a, me), rows(all_v, me)
+
+    def shifted(before, up, lanes):
+        ext = jnp.concatenate(
+            [before[:, lanes].astype(F32) * has_before, up[:, lanes].astype(F32)], 0
+        )
+        return [ext[HALO - reach + k : HALO - reach + k + length] for k in range(tap_count)]
+
+    def forward(at, carry):
+        lanes = pl.ds(pl.multiple_of(at * CHUNK, CHUNK), CHUNK)
+        taken_a, taken_v = shifted(before_a, up_a, lanes), shifted(before_v, up_v, lanes)
+        pre_a = jnp.broadcast_to(bias_a[:, lanes].astype(F32), (length, CHUNK))
+        pre_v = jnp.broadcast_to(bias_v[:, lanes].astype(F32), (length, CHUNK))
+        for k in range(tap_count):
+            pre_a = pre_a + taps_a[k : k + 1, lanes].astype(F32) * taken_a[k]
+            pre_v = pre_v + taps_v[k : k + 1, lanes].astype(F32) * taken_v[k]
+        square = pre_a * pre_a
+        bent = jnp.tanh(ROOT_TWO_OVER_PI * pre_a * (1.0 + CUBIC * square))
+        half = 0.5 * (1.0 + bent)
+        gelu = pre_a * half
+        slope = half + 0.5 * pre_a * (1.0 - bent * bent) * (
+            ROOT_TWO_OVER_PI * (1.0 + 3.0 * CUBIC * square)
+        )
+        out_m[:, lanes] = (gelu * pre_v).astype(BF16)
+        gated[:, lanes] = gelu
+        factor[:, lanes] = pre_v * slope
+        return carry
+
+    def spread(slot, ref):
+        pair = [
+            remote(10 + slot, rows(ref, me), rows(ref, me), send, receive, to(far)),
+            remote(13 + slot, rows(ref, me), rows(ref, me), send, receive, to(sib)),
+        ]
+        for copy in pair:
+            copy.start()
+        return pair
+
     partial(me, keep(own))
+    for copy in halo_copies:
+        copy.wait_recv()
+    lax.fori_loop(0, width // CHUNK, forward, 0)
+    spreads = [spread(0, all_m)]
     cot_copies[0].wait_recv()
     partial(sib, keep(to_sib))
     near_copy = remote(5, to_sib, from_sib, send, receive, to(sib))
@@ -108,42 +158,26 @@
     partial(far, add_far)
     far_copy = remote(7, to_far, from_far, send, receive, to(far))
     far_copy.start()
-    for copy in halo_copies:
-        copy.wait_recv()
+    relays = []
+
+    def relay_rows(slot, ref):
+        spreads[slot][0].wait_recv()
+        copy = remote(16 + slot, rows(ref, far), rows(ref, far), send, receive, to(sib))
+        copy.start()
+        relays.append(copy)
+
+    relay_rows(0, all_m)
     near_copy.wait_recv()
     far_copy.wait_recv()
 
-    has_before = (me > 0).astype(F32)
-    has_after = (me < count - 1).astype(F32)
-    out_m, out_a, out_v = rows(all_m, me), rows(all_a, me), rows(all_v, me)
-
-    def forward(at, carry):
+
+    def combine(at, carry):
         lanes = pl.ds(pl.multiple_of(at * CHUNK, CHUNK), CHUNK)
-        ext_a = jnp.concatenate(
-            [before_a[:, lanes].astype(F32) * has_before, up_a[:, lanes].astype(F32)], 0
-        )
-        ext_v = jnp.concatenate(
-            [before_v[:, lanes].astype(F32) * has_before, up_v[:, lanes].astype(F32)], 0
-        )
-        taken_a = [ext_a[HALO - reach + k : HALO - reach + k + length] for k in range(tap_count)]
-        taken_v = [ext_v[HALO - reach + k : HALO - reach + k + length] for k in range(tap_count)]
-        pre_a = jnp.broadcast_to(bias_a[:, lanes].astype(F32), (length, CHUNK))
-        pre_v = jnp.broadcast_to(bias_v[:, lanes].astype(F32), (length, CHUNK))
-        for k in range(tap_count):
-            pre_a = pre_a + taps_a[k : k + 1, lanes].astype(F32) * taken_a[k]
-            pre_v = pre_v + taps_v[k : k + 1, lanes].astype(F32) * taken_v[k]
-        square = pre_a * pre_a
-        bent = jnp.tanh(ROOT_TWO_OVER_PI * pre_a * (1.0 + CUBIC * square))
-        half = 0.5 * (1.0 + bent)
-        gelu = pre_a * half
-        slope = half + 0.5 * pre_a * (1.0 - bent * bent) * (
-            ROOT_TWO_OVER_PI * (1.0 + 3.0 * CUBIC * square)
-        )
-        out_m[:, lanes] = (gelu * pre_v).astype(BF16)
+        taken_a, taken_v = shifted(before_a, up_a, lanes), shifted(before_v, up_v, lanes)
         total = own[:, lanes] + from_sib[:, lanes].astype(F32) + from_far[:, lanes].astype(F32)
         grad_mixed = total.astype(BF16).astype(F32)
-        pre_grad_a = grad_mixed * pre_v * slope
-        pre_grad_v = grad_mixed * gelu
+        pre_grad_a = grad_mixed * factor[:, lanes]
+        pre_grad_v = grad_mixed * gated[:, lanes]
         grad_a[:, lanes] = pre_grad_a
         grad_v[:, lanes] = pre_grad_v
         found = [jnp.sum(pre_grad_a * taken, axis=0, keepdims=True) for taken in taken_a]
@@ -153,7 +187,7 @@
         own_sums[:, lanes] = jnp.concatenate(found, 0)
         return carry
 
-    lax.fori_loop(0, width // CHUNK, forward, 0)
+    lax.fori_loop(0, width // CHUNK, combine, 0)
     first = pl.ds(0, TAIL)
     back_copies = [
         remote(8, grad_a.at[first, :], after_a, send, receive, to(left)),
@@ -164,18 +198,8 @@
         for slot, peer in enumerate((sib, far, diag))
     ]
 
-    def spread(slot, ref):
-        pair = [
-            remote(10 + slot, rows(ref, me), rows(ref, me), send, receive, to(far)),
-            remote(13 + slot, rows(ref, me), rows(ref, me), send, receive, to(sib)),
-        ]
-        for copy in pair:
-            copy.start()
-        return pair
-
     for copy in back_copies:
         copy.start()
-    spreads = [spread(0, all_m)]
     for copy in sum_copies:
         copy.start()
 
@@ -197,18 +221,41 @@
     back_copies[1].wait_recv()
     backward(grad_v, after_v, taps_v, out_v)
     spreads.append(spread(2, all_v))
-    relays = []
-    for slot, (pair, ref) in enumerate(zip(spreads, (all_m, all_a, all_v))):
-        pair[0].wait_recv()
-        relay = remote(16 + slot, rows(ref, far), rows(ref, far), send, receive, to(sib))
-        relay.start()
-        relays.append(relay)
+
+    def add_terms(index, pairs, fresh):
+        span = pl.ds(pl.multiple_of(index * length, length), length)
+
+        def step(at, carry):
+            lanes = pl.ds(pl.multiple_of(at * CHUNK, CHUNK), CHUNK)
+            total = None if fresh else terms[span, lanes]
+            for ref, weights in pairs:
+                product = contract_last(ref[span, :], weights[lanes, :])
+                total = product if total is None else total + product
+            terms[span, lanes] = total
+            return carry
+
+        lax.fori_loop(0, depth // CHUNK, step, 0)
+
+    role_a, role_v = (all_a, held_a), (all_v, held_v)
+    for load in loads:
+        load.wait()
+    add_terms(me, (role_a, role_v), True)
+    spreads[1][1].wait_recv()
+    spreads[2][1].wait_recv()
+    add_terms(sib, (role_a, role_v), True)
+    relay_rows(1, all_a)
+    add_terms(far, (role_a,), True)
+    relays[1].wait_recv()
+    add_terms(diag, (role_a,), True)
+    relay_rows(2, all_v)
+    add_terms(far, (role_v,), False)
+    relays[2].wait_recv()
+    add_terms(diag, (role_v,), False)
     for copy in sum_copies:
         copy.wait_recv()
     sums[...] = (own_sums[...] + got_sums[0]) + (got_sums[1] + got_sums[2])
-    for pair, relay in zip(spreads, relays):
-        pair[1].wait_recv()
-        relay.wait_recv()
+    spreads[0][1].wait_recv()
+    relays[0].wait_recv()
     for copy in (
         *cot_copies, *halo_copies, near_copy, relay_copy, far_copy, *back_copies, *sum_copies,
         *(copy for pair in spreads for copy in pair), *relays,
@@ -216,7 +263,9 @@
         copy.wait_send()
 
 
-def gradients(cotangent, w_down, up_act, up_val, conv_act, conv_val, bias_act, bias_val):
+def gradients(
+    cotangent, w_down, up_act, up_val, conv_act, conv_val, bias_act, bias_val, w_act, w_val
+):
     length, width = up_act.shape
     depth = w_down.shape[1]
     tp_count = lax.axis_size("tp")
@@ -234,23 +283,26 @@
             jax.ShapeDtypeStruct((positions, width), BF16),
             jax.ShapeDtypeStruct((positions, width), BF16),
             jax.ShapeDtypeStruct((stat_rows, width), F32),
+            jax.ShapeDtypeStruct((positions, depth), F32),
         ),
-        in_specs=[vmem] * 8,
-        out_specs=(vmem,) * 5,
+        in_specs=[vmem] * 8 + [pl.BlockSpec(memory_space=pl.ANY)] * 2,
+        out_specs=(vmem,) * 6,
         scratch_shapes=[
             wide, block, block, block, block, block, block,
             pltpu.VMEM((HALO, width), BF16), pltpu.VMEM((HALO, width), BF16),
             wide, wide,
             pltpu.VMEM((TAIL, width), F32), pltpu.VMEM((TAIL, width), F32),
             pltpu.VMEM((stat_rows, width), F32), pltpu.VMEM((3, stat_rows, width), F32),
+            wide, wide, pltpu.VMEM(w_act.shape, BF16), pltpu.VMEM(w_val.shape, BF16),
             pltpu.SemaphoreType.DMA((22,)), pltpu.SemaphoreType.DMA((22,)),
+            pltpu.SemaphoreType.DMA((2,)),
         ],
         compiler_params=pltpu.CompilerParams(
             collective_id=0, has_side_effects=True, vmem_limit_bytes=50 * 1024 * 1024
         ),
     )(
         cotangent, w_down, up_act, up_val, conv_act, conv_val,
-        bias_act.reshape(1, width), bias_val.reshape(1, width),
+        bias_act.reshape(1, width), bias_val.reshape(1, width), w_act, w_val,
     )
 
 
@@ -396,12 +448,44 @@
         tp_count == 4
         and fs_count % 2 == 0
         and width % CHUNK == 0
-        and w_down.shape[1] % 128 == 0
+        and w_down.shape[1] % CHUNK == 0
         and length % (16 * fs_count) == 0
         and conv_act.shape[0] - 1 <= TAIL
         and conv_act.shape[0] == 3
-        and width * (w_down.shape[1] + 24 * length) * 2 <= 24 * 1024 * 1024
-    )
+        and width * (3 * w_down.shape[1] + 32 * length) * 2 <= 32 * 1024 * 1024
+    )
+
+
+def weight_kernel(left, right, out, norms):
+    value = contract_first(left[...], right[...])
+    out[...] = value
+    square = value * value
+    lanes = square[:, :128]
+    for at in range(128, square.shape[1], 128):
+        lanes = lanes + square[:, at : at + 128]
+    norms[...] = jnp.sum(lanes.T, axis=0, keepdims=True)
+
+
+def weight_gradient(left, right):
+    positions, height = left.shape
+    width = right.shape[1]
+    return pl.pallas_call(
+        weight_kernel,
+        grid=(height // CHUNK,),
+        out_shape=(
+            jax.ShapeDtypeStruct((height, width), F32),
+            jax.ShapeDtypeStruct((1, height), F32),
+        ),
+        in_specs=[
+            pl.BlockSpec((positions, CHUNK), lambda i: (0, i)),
+            pl.BlockSpec((positions, width), lambda i: (0, 0)),
+        ],
+        out_specs=(
+            pl.BlockSpec((CHUNK, width), lambda i: (i, 0)),
+            pl.BlockSpec((1, CHUNK), lambda i: (0, i)),
+        ),
+        compiler_params=pltpu.CompilerParams(vmem_limit_bytes=40 * 1024 * 1024),
+    )(left, right)
 
 
 def with_kernels(
@@ -409,13 +493,12 @@
     conv_act, conv_val, bias_act, bias_val,
 ):
     tap_count = conv_act.shape[0]
-    cot_columns, all_up_act, all_up_val, all_mixed, sums = gradients(
-        cotangent, w_down, up_act, up_val, conv_act, conv_val, bias_act, bias_val
-    )
-    grad_w_act = contract_first(hidden_in, all_up_act)
-    grad_w_val = contract_first(hidden_in, all_up_val)
-    grad_w_down = contract_first(all_mixed, cot_columns)
-    terms = contract_last(all_up_act, w_act) + contract_last(all_up_val, w_val)
+    cot_columns, all_up_act, all_up_val, all_mixed, sums, terms = gradients(
+        cotangent, w_down, up_act, up_val, conv_act, conv_val, bias_act, bias_val, w_act, w_val
+    )
+    grad_w_act, act_norms = weight_gradient(hidden_in, all_up_act)
+    grad_w_val, val_norms = weight_gradient(hidden_in, all_up_val)
+    grad_w_down, down_norms = weight_gradient(all_mixed, cot_columns)
     taps_act, sums_act = sums[:tap_count], sums[tap_count]
     taps_val, sums_val = sums[tap_count + 1 : 2 * tap_count + 1], sums[2 * tap_count + 1]
     tap_squares = jnp.stack(
@@ -425,14 +508,14 @@
     flat = tap_squares.reshape(1, -1)
     stat = jnp.concatenate(
         [
-            jnp.sum(grad_w_act * grad_w_act, axis=1)[None],
-            jnp.sum(grad_w_val * grad_w_val, axis=1)[None],
+            act_norms,
+            val_norms,
             jnp.pad(flat, ((0, 0), (0, depth - flat.shape[1]))),
             jnp.zeros((5, depth), F32),
         ],
         0,
     )
-    down_stat = jnp.pad(jnp.sum(grad_w_down * grad_w_down, axis=1)[None], ((0, 7), (0, 0)))
+    down_stat = jnp.pad(down_norms, ((0, 7), (0, 0)))
     grad_input, stat, down_stat = reduced(terms, stat, down_stat)
     return (
         grad_input,

time: 153 us -> 127 us (0.83)
  matrix products: 20.1 us -> 0 us
  local copies, waits for them, and re-layouts: 32.6 us -> 16.4 us
  Pallas kernels: 97.3 us -> 108 us
    dot_general x5 -> x0, matrix products: 20.1 us -> none  [the longest x3 13.6 us: contract_first(): lax.dot_general(left, right, (((0,), (0,)), ((), ())), preferred_element_...]
    unnamed x32 -> x23, local copies, waits for them, and re-layouts: 26 us -> 9.99 us
    pallas_call x0 -> x3, Pallas kernels: none -> 13.5 us  [weight_gradient(): pl.pallas_call(weight_kernel, grid=(height // CHUNK,), out_shape=(jax.Sha...]
    pallas_call x1, Pallas kernels: 69.2 us -> 65.2 us  [gradients(): pl.pallas_call(gradient_kernel, out_shape=(jax.ShapeDtypeStruct((position...]
where the time goes in v2:
time: 127 us
  Pallas kernels  108 us (85%)
  local copies, waits for them, and re-layouts  16.4 us (13%)
  other arithmetic  1.45 us (1%)
    pallas_call x1, Pallas kernels, gradients(): pl.pallas_call(gradient_kernel, out_shape=(jax.ShapeDtypeStruct((position...  65.2 us
    pallas_call x1, Pallas kernels, reduced(): pl.pallas_call(reduce_kernel, out_shape=(jax.ShapeDtypeStruct((shard, dep...  29.5 us
    pallas_call x3, Pallas kernels, weight_gradient(): pl.pallas_call(weight_kernel, grid=(height // CHUNK,), out_shape=(jax.Sha...  13.5 us
    unnamed x23, local copies, waits for them, and re-layouts  9.99 us

profile of v2, /device:TPU:0, one launch (start us, length us, event | category | flops | bytes accessed | tf_op | source)
XLA Modules:
  0.0 126.7 jit_solution(7074540574220929578)
XLA Ops:
  0.7 0.1 pad.13.clone
  0.7 0.7 reshape.33.bias_a
  1.4 0.7 reshape.34.bias_v
  2.1 0.0 copy-start.4
  2.1 1.2 copy-done.4
  3.3 0.0 copy-start.7
  3.3 1.0 copy-done.7
  4.3 0.0 copy-start.8
  4.3 1.0 copy-done.8
  5.3 0.0 copy-start.9
  5.3 0.7 copy-done.9
  6.0 0.0 copy-start.10
  6.0 0.7 copy-done.10
  6.7 0.0 copy-start
  6.7 65.2 %shard_map.202 = (bf16[512,1024]{1,0:T(8,128)(2,1)S(1)}, bf16[512,1536]{1,0:T(8,128)(2,1)}, bf16[512,1536]{1,0:T(8,128)(2,1)}, bf16[512,1536]{1,0:T(8,128)(2,1)}...) custom-call(bf16[128,4096]{1,0:T(8,128)(2,1)S(1)} %copy-done.4, bf16[1536,1024]{1,0:T(8,128)(2,1)} %down.1, ...), custom_call_target="tpu_custom_call" | custom-call | tf_op jit(solution)/shard_map/pallas_call | solution.py:278
  71.9 0.0 copy-start.5
  71.9 1.0 copy-done.5
  72.9 0.0 copy-start.1
  72.9 0.8 multiply_reduce_fusion.1
  73.7 0.1 reshape.35
  73.7 0.0 copy-done
  73.8 0.0 copy-start.3
  73.8 1.4 %copy-done.3 = bf16[512,1536]{1,0:T(8,128)(2,1)S(1)} copy-done((bf16[512,1536]{1,0:T(8,128)(2,1)S(1)}, bf16[512,1536]{1,0:T(8,128)(2,1)}, u32[]{:S(2)}) %copy-start.3) | copy-done | bytes 1572888
  75.2 0.0 copy-start.6
  75.2 4.3 %shard_map.203 = (f32[1024,1536]{1,0:T(8,128)}, f32[1,1024]{1,0:T(1,128)S(1)}) custom-call(bf16[512,1024]{1,0:T(8,128)(2,1)S(1)} %copy-done, bf16[512,1536]{1,0:T(8,128)(2,1)S(1)} %copy-done.3), custom_call_target="tpu_custom_call" | custom-call | tf_op jit(solution)/shard_map/pallas_call | solution.py:472
  79.5 0.0 copy-start.2
  79.5 1.4 %copy-done.2 = bf16[512,1536]{1,0:T(8,128)(2,1)S(1)} copy-done((bf16[512,1536]{1,0:T(8,128)(2,1)S(1)}, bf16[512,1536]{1,0:T(8,128)(2,1)}, u32[]{:S(2)}) %copy-start.2) | copy-done | bytes 1572888
  80.9 4.3 %shard_map.204 = (f32[1024,1536]{1,0:T(8,128)}, f32[1,1024]{1,0:T(1,128)S(1)}) custom-call(bf16[512,1024]{1,0:T(8,128)(2,1)S(1)} %copy-done, bf16[512,1536]{1,0:T(8,128)(2,1)S(1)} %copy-done.2), custom_call_target="tpu_custom_call" | custom-call | tf_op jit(solution)/shard_map/pallas_call | solution.py:472
  85.1 0.7 fusion.stat
  85.8 0.0 copy-done.1
  85.8 0.0 copy-done.6
  85.8 4.9 %shard_map.205 = (f32[1536,1024]{1,0:T(8,128)}, f32[1,1536]{1,0:T(1,128)S(1)}) custom-call(bf16[512,1536]{1,0:T(8,128)(2,1)S(1)} %copy-done.1, bf16[512,1024]{1,0:T(8,128)(2,1)S(1)} %copy-done.6), custom_call_target="tpu_custom_call" | custom-call | tf_op jit(solution)/shard_map/pallas_call | solution.py:472
  90.8 0.6 pad.9.down_stat
  91.4 29.5 %shard_map.206 = (bf16[16,4096]{1,0:T(8,128)(2,1)}, f32[8,1024]{1,0:T(8,128)}, f32[8,1536]{1,0:T(8,128)}) custom-call(f32[512,1024]{1,0:T(8,128)} %get-tuple-element.27.terms, f32[8,1024]{1,0:T(8,128)} %fusion.stat, f32[8,1536]{1,0:T(8,128)} %pad.9.down_stat), custom_call_target="tpu_custom_call" | custom-call | tf_op jit(solution)/shard_map/pallas_call | solution.py:424
  120.9 1.5 %slice_reduce_fusion.1 = (f32[1536]{0:T(1024)}, f32[1536]{0:T(1024)}, f32[1536]{0:T(1024)}) fusion(f32[8,1536]{1,0:T(8,128)S(1)} %get-tuple-element.32, f32[8,1536]{1,0:T(8,128)} %get-tuple-element.41), kind=kLoop, calls=%fused_computation.8 | loop fusion | bytes 36864 | tf_op jit(solution)/shard_map/slice | solution.py:503
  122.3 0.7 slice_reduce_fusion.3
  123.0 1.4 %fusion.2 = (f32[1,1024]{1,0:T(1,128)}, f32[1,1024]{1,0:T(1,128)}) fusion(f32[8,1024]{1,0:T(8,128)} %get-tuple-element.40), kind=kLoop, calls=%fused_computation.12 | loop fusion | bytes 16384 | tf_op jit(solution)/shard_map/slice | solution.py:530
  124.5 0.6 reshape_squeeze.3
  125.1 1.6 %copy.24 = bf16[16,4096]{1,0:T(8,128)(2,1)} copy(bf16[16,4096]{1,0:T(8,128)(2,1)} %get-tuple-element.65) | data formatting | bytes 262144
  (2 shorter events, 0.0 us)
Async XLA Ops:
  2.1 1.2 copy-start.4
  3.3 1.0 copy-start.7
  4.3 1.0 copy-start.8
  5.3 0.7 copy-start.9
  6.0 0.7 copy-start.10
  6.7 67.0 %copy-start = (bf16[512,1024]{1,0:T(8,128)(2,1)S(1)}, bf16[512,1024]{1,0:T(8,128)(2,1)}, u32[]{:S(2)}) copy-start(bf16[512,1024]{1,0:T(8,128)(2,1)} %left.3) | copy-start | bytes 3145732
  71.9 1.0 copy-start.5
  72.9 12.9 %copy-start.1 = (bf16[512,1536]{1,0:T(8,128)(2,1)S(1)}, bf16[512,1536]{1,0:T(8,128)(2,1)}, u32[]{:S(2)}) copy-start(bf16[512,1536]{1,0:T(8,128)(2,1)} %get-tuple-element.33.left) | copy-start | bytes 4718596
  73.8 1.4 %copy-start.3 = (bf16[512,1536]{1,0:T(8,128)(2,1)S(1)}, bf16[512,1536]{1,0:T(8,128)(2,1)}, u32[]{:S(2)}) copy-start(bf16[512,1536]{1,0:T(8,128)(2,1)} %get-tuple-element.28.right) | copy-start | bytes 4718596
  75.2 10.7 %copy-start.6 = (bf16[512,1024]{1,0:T(8,128)(2,1)S(1)}, bf16[512,1024]{1,0:T(8,128)(2,1)}, u32[]{:S(2)}) copy-start(bf16[512,1024]{1,0:T(8,128)(2,1)} %copy-done.5) | copy-start | bytes 3145732
  79.5 1.4 %copy-start.2 = (bf16[512,1536]{1,0:T(8,128)(2,1)S(1)}, bf16[512,1536]{1,0:T(8,128)(2,1)}, u32[]{:S(2)}) copy-start(bf16[512,1536]{1,0:T(8,128)(2,1)} %get-tuple-element.30.right) | copy-start | bytes 4718596
